TPU v7x, 32 devices: a whole 2x2x4 slice. The times are simulated.
32 devices in a mesh: grp: 2 (over x), ep: 16 (over z, y, core).
Axes of the slice: x: 2, y: 2, z: 4, core: 2. Of those that a mesh axis runs over, the one named last changes fastest.
Arguments:
- stream: bfloat16 [32, 2048], P('grp', 'ep'), parts along dimension 0, may hold values from -48 to 48
- conv_cache: bfloat16 [32, 3, 2560], P(('grp', 'ep')), parts along dimension 0, may hold values from -6 to 6
- scan_state: float32 [32, 32, 64, 128], P(('grp', 'ep')), parts along dimension 0, may hold values from -4 to 4
- gate_weight: bfloat16 [2048, 2048], P('ep'), may hold values from -0.125 to 0.125
- value_weight: bfloat16 [2048, 2048], P('ep'), may hold values from -0.125 to 0.125
- entry_weight: bfloat16 [2048, 256], P('ep'), may hold values from -0.125 to 0.125
- readout_weight: bfloat16 [2048, 256], P('ep'), may hold values from -0.125 to 0.125
- step_weight: bfloat16 [2048, 32], P('ep'), may hold values from -0.125 to 0.125
- conv_weight: bfloat16 [4, 2560], replicated, may hold values from -3 to 3
- step_bias: float32 [32], replicated, may hold values from -4 to -1
- decay_rate: float32 [32], replicated, may hold values from 0.5 to 8
- skip_gain: float32 [32], replicated, may hold values from 0.1 to 1.9
- group_gain: float32 [2048], replicated, may hold values from 0.1 to 1.9
- out_weight: bfloat16 [2048, 2048], P(None, 'ep'), may hold values from -0.125 to 0.125
- first_gain: float32 [2048], replicated, may hold values from 0.1 to 1.9
- routes: int32 [32, 4], P('grp'), parts along dimension 0, may hold values from 0 to 15, all different within a row; in each aligned block of 16 rows (0 to 15, 16 to 31, ...) at most 8 rows name the same one
- route_weight: float32 [32, 4], P('grp'), parts along dimension 0, may hold values from 0.1 to 1
- expert_gate: bfloat16 [16, 2048, 256], P('ep'), may hold values from -0.125 to 0.125
- expert_up: bfloat16 [16, 2048, 256], P('ep'), may hold values from -0.125 to 0.125
- expert_down: bfloat16 [16, 256, 2048], P('ep'), may hold values from -0.375 to 0.375
- shared_gate: bfloat16 [2048, 256], replicated, may hold values from -0.125 to 0.125
- shared_up: bfloat16 [2048, 256], replicated, may hold values from -0.125 to 0.125
- shared_down: bfloat16 [256, 2048], replicated, may hold values from -0.375 to 0.375
- second_gain: float32 [2048], P('ep'), may hold values from 0.1 to 1.9
Outputs:
- result: bfloat16 [32, 2048], P('grp', 'ep'), parts along dimension 0
- new_conv: bfloat16 [32, 3, 2560], P(('grp', 'ep')), parts along dimension 0
- new_state: float32 [32, 32, 64, 128], P(('grp', 'ep')), parts along dimension 0
There are 2 independent parts, one for each index of `grp`. A program takes and returns all parts, laid end to end along the dimension named above; an argument that names none is the same for every part. Nothing has to cross between parts.
Inputs may be any that keep to these rules, and one draw needn't show every extreme that they name: `routes`: each row names 4 different experts; no expert is named by more than 8 rows, a bound that some block reaches.
All inputs are finite; a program needn't handle non-finite values.
Results may differ from a plain program's by a relative error of at most 0.0065.
Values may be sent and summed in bfloat16 or wider, within the bound.
A program may use at most 64 MiB of HBM per device.

v0:
```python
import jax
import jax.numpy as jnp
from jax import lax
from jax.sharding import PartitionSpec as P

HEAD_DIM = 64
STATE = 128
GROUPS = 2
CAP = 8
RESIDUAL_SCALE = 2.0**0.25
NORM_EPSILON = 1e-05
GATED_EPSILON = 1e-06


def rounded(value):
    return lax.optimization_barrier(value.astype(jnp.bfloat16))


def finish_norm(residual, row_total, square, full_width, gain):
    mean_value = (row_total / full_width)[:, None]
    variance = (square / full_width)[:, None] - mean_value * mean_value
    return (residual - mean_value) * lax.rsqrt(variance + NORM_EPSILON) * gain


def swiglu(inputs, gate_matrix, up_matrix, down_matrix):
    hidden = (
        jax.nn.silu(jnp.dot(inputs, gate_matrix, preferred_element_type=jnp.float32))
        * jnp.dot(inputs, up_matrix, preferred_element_type=jnp.float32)
    ).astype(jnp.bfloat16)
    return rounded(jnp.dot(hidden, down_matrix, preferred_element_type=jnp.float32))


def on_device(
    stream,
    conv_cache,
    scan_state,
    gate_weight,
    value_weight,
    entry_weight,
    readout_weight,
    step_weight,
    conv_weight,
    step_bias,
    decay_rate,
    skip_gain,
    group_gain,
    out_weight,
    first_gain,
    routes,
    route_weight,
    expert_gate,
    expert_up,
    expert_down,
    shared_gate,
    shared_up,
    shared_down,
    second_gain,
):
    devices = lax.axis_size("ep")
    device_rank = lax.axis_index("ep")
    own_rows = conv_cache.shape[0]
    row_count = stream.shape[0]
    slice_width = stream.shape[1]
    full_width = slice_width * devices
    inner_width = gate_weight.shape[1]
    head_count = step_weight.shape[1]
    per_group = head_count // GROUPS
    group_width = inner_width // GROUPS
    bounds = (inner_width, 2 * inner_width + 2 * GROUPS * STATE)
    weights_in = (gate_weight, value_weight, entry_weight, readout_weight, step_weight)
    summed = rounded(
        lax.psum_scatter(
            jnp.concatenate(
                [
                    jnp.dot(stream, weight, preferred_element_type=jnp.float32)
                    for weight in weights_in
                ],
                axis=1,
            ),
            "ep",
            scatter_dimension=0,
            tiled=True,
        )
    )
    gate_rows = summed[:, : bounds[0]]
    fresh = summed[:, bounds[0] : bounds[1]]
    step_rows = summed[:, bounds[1] :]
    window = jnp.concatenate([conv_cache, fresh[:, None, :]], axis=1)
    active = jax.nn.silu(
        jnp.sum(window.astype(jnp.float32) * conv_weight.astype(jnp.float32)[None], axis=1)
    )
    head_in = active[:, :inner_width].reshape(own_rows, GROUPS, per_group, HEAD_DIM)
    entry_rows = active[:, inner_width : inner_width + GROUPS * STATE].reshape(
        own_rows, GROUPS, 1, 1, STATE
    )
    readout_rows = active[:, inner_width + GROUPS * STATE :].reshape(own_rows, GROUPS, 1, 1, STATE)
    step_size = jax.nn.softplus(step_rows.astype(jnp.float32) + step_bias).reshape(
        own_rows, GROUPS, per_group
    )
    retained = jnp.exp(-step_size * decay_rate.reshape(GROUPS, per_group))
    old_state = scan_state.reshape(own_rows, GROUPS, per_group, HEAD_DIM, STATE)
    new_state = (
        retained[..., None, None] * old_state
        + (step_size[..., None] * head_in)[..., None] * entry_rows
    )
    head_out = (
        jnp.sum(new_state * readout_rows, axis=-1)
        + skip_gain.reshape(GROUPS, per_group)[:, :, None] * head_in
    )
    gated_out = head_out.reshape(own_rows, GROUPS, group_width) * jax.nn.silu(
        gate_rows.astype(jnp.float32)
    ).reshape(own_rows, GROUPS, group_width)
    normed = gated_out * lax.rsqrt(
        jnp.mean(gated_out * gated_out, axis=-1, keepdims=True) + GATED_EPSILON
    )
    normed = (normed.reshape(own_rows, inner_width) * group_gain).astype(jnp.bfloat16)
    mixer_out = rounded(
        jnp.dot(
            lax.all_gather(normed, "ep", axis=0, tiled=True),
            out_weight,
            preferred_element_type=jnp.float32,
        )
    )
    column_start = device_rank * slice_width
    residual = RESIDUAL_SCALE * stream.astype(jnp.float32) + mixer_out.astype(jnp.float32)
    row_total, square = lax.psum(
        (jnp.sum(residual, axis=1), jnp.sum(residual * residual, axis=1)), "ep"
    )
    gain_part = lax.dynamic_slice_in_dim(first_gain, column_start, slice_width, 0)
    first_part = rounded(finish_norm(residual, row_total, square, full_width, gain_part))
    first_rows = lax.all_gather(first_part, "ep", axis=1, tiled=True)
    matches = routes[:, :, None] == jnp.arange(devices, dtype=jnp.int32)[None, None, :]
    member = jnp.sum(matches.astype(jnp.int32), axis=1)
    weight_of = jnp.sum(jnp.where(matches, route_weight[:, :, None], 0.0), axis=1)
    slot_rank = jnp.cumsum(member, axis=0) - member
    slot_ids = jnp.arange(CAP, dtype=jnp.int32)
    mine_member = lax.dynamic_slice_in_dim(member, device_rank, 1, 1)[:, 0]
    mine_slot = lax.dynamic_slice_in_dim(slot_rank, device_rank, 1, 1)[:, 0]
    chosen = (mine_slot[None, :] == slot_ids[:, None]) & (mine_member[None, :] == 1)
    taken_rows = jnp.dot(
        chosen.astype(jnp.bfloat16), first_rows, preferred_element_type=jnp.float32
    ).astype(jnp.bfloat16)
    expert_out = swiglu(taken_rows, expert_gate[0], expert_up[0], expert_down[0])
    arrived = lax.all_to_all(expert_out, "ep", split_axis=1, concat_axis=0, tiled=True)
    spread = jnp.where(
        (slot_rank[:, :, None] == slot_ids[None, None, :]) & (member[:, :, None] == 1),
        weight_of[:, :, None],
        0.0,
    )
    moe_part = jnp.dot(
        spread.reshape(row_count, devices * CAP),
        arrived.astype(jnp.float32),
        precision=lax.Precision.HIGHEST,
    )
    down_part = lax.dynamic_slice_in_dim(shared_down, column_start, slice_width, 1)
    shared_part = swiglu(first_rows, shared_gate, shared_up, down_part)
    moe_part = moe_part + shared_part.astype(jnp.float32)
    residual_two = RESIDUAL_SCALE * first_part.astype(jnp.float32) + moe_part
    total_two, square_two = lax.psum(
        (jnp.sum(residual_two, axis=1), jnp.sum(residual_two * residual_two, axis=1)), "ep"
    )
    result = finish_norm(residual_two, total_two, square_two, full_width, second_gain).astype(
        jnp.bfloat16
    )
    return (result, window[:, 1:], new_state.reshape(own_rows, head_count, HEAD_DIM, STATE))


def solution(mesh):
    return jax.shard_map(
        on_device,
        mesh=mesh,
        in_specs=(
            P("grp", "ep"),
            P(("grp", "ep"), None, None),
            P(("grp", "ep"), None, None, None),
            P("ep", None),
            P("ep", None),
            P("ep", None),
            P("ep", None),
            P("ep", None),
            P(),
            P(),
            P(),
            P(),
            P(),
            P(None, "ep"),
            P(),
            P("grp", None),
            P("grp", None),
            P("ep", None, None),
            P("ep", None, None),
            P("ep", None, None),
            P(),
            P(),
            P(),
            P("ep"),
        ),
        out_specs=(
            P("grp", "ep"),
            P(("grp", "ep"), None, None),
            P(("grp", "ep"), None, None, None),
        ),
        check_vma=False,
    )
```

profile of v0, /device:TPU:0, one launch (start us, length us, event | category | flops | bytes accessed | tf_op | source)
XLA Modules:
  0.0 191.0 jit_solution(8677031213126030681)
XLA Ops:
  0.6 0.0 copy-start
  0.7 0.7 copy-done.7
  1.4 1.3 convolution_dynamic-update-slice_fusion.1
  2.7 0.2 convolution_dynamic-update-slice_fusion
  2.9 1.0 convolution_dynamic-update-slice_fusion.3
  3.9 1.0 convolution_dynamic-update-slice_fusion.2
  4.9 0.8 convolution_dynamic-update-slice_fusion.4
  5.7 66.2 %all-reduce.4 = bf16[16,4640]{1,0:T(8,128)(2,1)S(1)} all-reduce(f32[16,4640]{1,0:T(8,128)S(1)} %convolution_dynamic-update-slice_fusion.4), channel_id=3, replica_groups=mesh['grp'=2,'ep'=16] {'ep'}, use_global_device_ids=true, to_apply=%region_0.0.clone | all-reduce | flops 74240 | bytes 445440
  71.9 0.0 copy-start.17
  71.9 0.6 copy-done.17
  72.6 0.6 dynamic-slice
  73.1 0.7 dynamic-slice_convert_fusion
  73.8 0.0 copy-start.8
  73.9 0.0 copy-done.9
  73.9 0.7 copy-done.8
  74.6 0.1 multiply_reduce_fusion.1
  74.7 0.0 copy-start.14
  74.7 0.0 copy-start.15
  74.7 0.1 reshape.257
  74.8 0.6 copy-done.14
  75.4 0.0 copy-done.15
  75.4 0.1 broadcast_multiply_fusion
  75.5 0.0 copy-done.1
  75.5 0.0 copy-start.16
  75.5 0.0 copy-start.11
  75.5 1.4 multiply_reduce_fusion
  76.9 0.1 reduce_sum.91
  77.0 0.1 reduce_sum.90
  77.0 0.1 mul.271
  77.1 0.1 mul.272
  77.2 0.1 mul.277
  77.3 0.1 mul.273
  77.4 0.5 broadcast.167
  77.9 0.7 fusion.47
  78.6 0.1 multiply_reduce_fusion.4
  78.7 0.1 mul.281
  78.8 0.0 copy-start.10
  78.8 17.3 %all-gather = bf16[32768]{0:T(1024)(128)(2,1)S(1)} all-gather(bf16[2048]{0:T(1024)(128)(2,1)S(1)} %multiply_convert_fusion.2), channel_id=2, replica_groups=mesh['grp'=2,'ep'=16] {'ep'}, dimensions={0}, use_global_device_ids=true | all-gather | bytes 69632 | tf_op jit(solution)/shard_map/all_gather | solution.py:119
  96.2 1.3 convolution_convert_fusion.2
  97.5 0.1 fusion.33
  97.6 0.8 dynamic_slice.12
  98.4 31.4 %all-reduce.2 = (f32[16]{0:T(128)S(1)}, f32[16]{0:T(128)S(1)}) all-reduce(f32[16]{0:T(128)S(1)} %get-tuple-element.6, f32[16]{0:T(128)S(1)} %get-tuple-element.5), channel_id=1, replica_groups=mesh['grp'=2,'ep'=16] {'ep'}, use_global_device_ids=true, to_apply=%region_7.8 | all-reduce | flops 32 | bytes 256 | tf_op jit(solution)/shard_map/psum | solution.py:126
  129.8 0.1 multiply_convert_fusion.1
  129.9 17.3 %all_gather.7 = bf16[16,2048]{1,0:T(8,128)(2,1)S(1)} all-gather(bf16[16,128]{1,0:T(8,128)(2,1)S(1)} %multiply_convert_fusion.1), channel_id=1, replica_groups=mesh['grp'=2,'ep'=16] {'ep'}, dimensions={1}, use_global_device_ids=true | all-gather | bytes 69632 | tf_op jit(solution)/shard_map/all_gather | solution.py:131
  147.2 0.0 copy-done.10
  147.2 0.1 convert_reduce_fusion
  147.3 0.2 fusion.32
  147.5 0.2 dynamic-slice_reduce_fusion
  147.6 0.1 convolution_convert_fusion.1
  147.8 0.2 fusion.9
  148.0 0.0 copy-done
  148.0 0.0 copy-start.4
  148.1 1.3 convolution_convert_fusion
  149.4 3.6 %all-to-all-start = ((bf16[8,16,128]{2,0,1:T(8,128)(2,1)}), bf16[8,16,128]{2,0,1:T(8,128)(2,1)S(1)}, u32[]{:S(2)}, u32[]{:S(2)}) async-start(bf16[8,16,128]{2,0,1:T(8,128)(2,1)} %bitcast.13), calls=%async_computation | async-start | bytes 65536 | tf_op jit(solution)/shard_map/all_to_all | solution.py:144
  153.0 0.2 fusion.50
  153.3 1.2 fusion.5
  154.5 0.7 pad_maximum_fusion
  155.2 0.0 copy-done.12
  155.2 0.1 select_reduce_fusion
  155.3 4.3 %all-to-all-done = bf16[8,16,128]{2,0,1:T(8,128)(2,1)S(1)} async-done(((bf16[8,16,128]{2,0,1:T(8,128)(2,1)}), bf16[8,16,128]{2,0,1:T(8,128)(2,1)S(1)}, u32[]{:S(2)}, u32[]{:S(2)}) %all-to-all-start) | async-done | bytes 32800 | tf_op jit(solution)/shard_map/all_to_all | solution.py:144
  159.6 0.4 fusion.45
  160.0 29.7 %all-reduce.1 = (f32[16]{0:T(128)S(1)}, f32[16]{0:T(128)S(1)}) all-reduce(f32[16]{0:T(128)S(1)} %get-tuple-element.4, f32[16]{0:T(128)S(1)} %get-tuple-element.3), channel_id=1, replica_groups=mesh['grp'=2,'ep'=16] {'ep'}, use_global_device_ids=true, to_apply=%region_14.15 | all-reduce | flops 32 | bytes 256 | tf_op jit(solution)/shard_map/psum | solution.py:159
  189.7 0.7 copy-done.13
  190.3 0.7 multiply_convert_fusion
  (33 shorter events, 0.3 us)
Async XLA Ops:
  0.6 147.4 %copy-start = (bf16[1,256,2048]{2,1,0:T(8,128)(2,1)S(1)}, bf16[1,256,2048]{2,1,0:T(8,128)(2,1)}, u32[]{:S(2)}) copy-start(bf16[1,256,2048]{2,1,0:T(8,128)(2,1)} %param.43) | copy-start | bytes 3145732
  0.6 0.8 copy-start.7
  0.7 2.1 %copy-start.6 = (bf16[128,2048]{1,0:T(8,128)(2,1)S(1)}, bf16[128,2048]{1,0:T(8,128)(2,1)}, u32[]{:S(2)}) copy-start(bf16[128,2048]{1,0:T(8,128)(2,1)} %param.28) | copy-start | bytes 1572868
  1.4 74.1 %copy-start.1 = (f32[1,32,64,128]{3,2,1,0:T(8,128)S(1)}, f32[1,32,64,128]{3,2,1,0:T(8,128)}, u32[]{:S(2)}) copy-start(f32[1,32,64,128]{3,2,1,0:T(8,128)} %param.26) | copy-start | bytes 3145732
  71.9 0.7 copy-start.17
  73.1 0.7 copy-start.9
  73.8 0.7 copy-start.8
  74.7 0.7 copy-start.14
  74.7 0.7 copy-start.15
  75.5 1.6 copy-start.16
  75.5 3.3 %copy-start.11 = (f32[2048]{0:T(1024)S(1)}, f32[2048]{0:T(1024)}, u32[]{:S(2)}) copy-start(f32[2048]{0:T(1024)} %param.36) | copy-start | bytes 24580
  76.9 70.9 %copy-start.2 = (bf16[1,2048,256]{2,1,0:T(8,128)(2,1)S(1)}, bf16[1,2048,256]{2,1,0:T(8,128)(2,1)}, u32[]{:S(2)}) copy-start(bf16[1,2048,256]{2,1,0:T(8,128)(2,1)} %param.41) | copy-start | bytes 3145732
  78.8 68.3 %copy-start.10 = (s32[16,4]{0,1:T(4,128)S(1)}, s32[16,4]{0,1:T(4,128)}, u32[]{:S(2)}) copy-start(s32[16,4]{0,1:T(4,128)} %param.39) | copy-start | bytes 772
  96.1 51.9 %copy-start.3 = (bf16[1,2048,256]{2,1,0:T(8,128)(2,1)S(1)}, bf16[1,2048,256]{2,1,0:T(8,128)(2,1)}, u32[]{:S(2)}) copy-start(bf16[1,2048,256]{2,1,0:T(8,128)(2,1)} %param.42) | copy-start | bytes 3145732
  148.0 5.0 %copy-start.4 = (bf16[2048,256]{1,0:T(8,128)(2,1)S(1)}, bf16[2048,256]{1,0:T(8,128)(2,1)}, u32[]{:S(2)}) copy-start(bf16[2048,256]{1,0:T(8,128)(2,1)} %param.44) | copy-start | bytes 3145732
  149.4 3.9 %copy-start.5 = (bf16[2048,256]{1,0:T(8,128)(2,1)S(1)}, bf16[2048,256]{1,0:T(8,128)(2,1)}, u32[]{:S(2)}) copy-start(bf16[2048,256]{1,0:T(8,128)(2,1)} %param.45) | copy-start | bytes 3145732
  149.4 10.2 %all-to-all-start = ((bf16[8,16,128]{2,0,1:T(8,128)(2,1)}), bf16[8,16,128]{2,0,1:T(8,128)(2,1)S(1)}, u32[]{:S(2)}, u32[]{:S(2)}) async-start(bf16[8,16,128]{2,0,1:T(8,128)(2,1)} %bitcast.13), calls=%async_computation | async-start | bytes 65536 | tf_op jit(solution)/shard_map/all_to_all | solution.py:144
  154.5 0.7 copy-start.12
  189.7 0.7 copy-start.13
where the time goes:
time: 192 us; the launch traced here: 191 us
  blocking collectives  162 us (84%)
  matrix products  9.08 us (5%)
  local copies, waits for them, and re-layouts  6.89 us (4%)
  waiting for transfers between devices  4.33 us (2%)
  other arithmetic  4.32 us (2%)
  starting transfers between devices  3.63 us (2%)
    unnamed x1, blocking collectives  66.2 us
    psum x1, blocking collectives, on_device(): lax.psum((jnp.sum(residual, axis=1), jnp.sum(residual * residual, axis=1)...  31.4 us
    psum x1, blocking collectives, on_device(): lax.psum((jnp.sum(residual_two, axis=1), jnp.sum(residual_two * residual_...  29.7 us
    all_gather x1, blocking collectives, on_device(): lax.all_gather(normed, 'ep', axis=0, tiled=True)  17.3 us
    all_gather x1, blocking collectives, on_device(): first_rows = lax.all_gather(first_part, 'ep', axis=1, tiled=True)  17.3 us
    all_to_all x1, waiting for transfers between devices, on_device(): lax.all_to_all(expert_out, 'ep', split_axis=1, concat_axis=0, tiled=True)  4.33 us
    dot_general x5, matrix products, on_device(): jnp.dot(stream, weight, preferred_element_type=jnp.float32)  4.26 us
    unnamed x37, local copies, waits for them, and re-layouts  4.03 us
  transfers between devices with their start and end apart: 1, of which 1 were waited for; matrix products, arithmetic and copies ran while one was open for 1% of the time, Pallas kernels for 0%

commit v1 on v0

--- a/solution.py
+++ b/solution.py
@@ -128,7 +128,7 @@
     )
     gain_part = lax.dynamic_slice_in_dim(first_gain, column_start, slice_width, 0)
     first_part = rounded(finish_norm(residual, row_total, square, full_width, gain_part))
-    first_rows = lax.all_gather(first_part, "ep", axis=1, tiled=True)
+    first_rows = jnp.concatenate(lax.all_gather(first_part, "ep"), axis=1)
     matches = routes[:, :, None] == jnp.arange(devices, dtype=jnp.int32)[None, None, :]
     member = jnp.sum(matches.astype(jnp.int32), axis=1)
     weight_of = jnp.sum(jnp.where(matches, route_weight[:, :, None], 0.0), axis=1)

time: 192 us -> 191 us (level)
  no operation moved by 1% of the time
where the time goes in v1:
time: 191 us; the launch traced here: 190 us
  blocking collectives  162 us (85%)
  matrix products  9.17 us (5%)
  local copies, waits for them, and re-layouts  6.16 us (3%)
  waiting for transfers between devices  4.33 us (2%)
  other arithmetic  4.31 us (2%)
  starting transfers between devices  3.63 us (2%)
    unnamed x1, blocking collectives  66.2 us
    psum x1, blocking collectives, on_device(): lax.psum((jnp.sum(residual, axis=1), jnp.sum(residual * residual, axis=1)...  31.4 us
    psum x1, blocking collectives, on_device(): lax.psum((jnp.sum(residual_two, axis=1), jnp.sum(residual_two * residual_...  29.7 us
    all_gather x1, blocking collectives, on_device(): lax.all_gather(normed, 'ep', axis=0, tiled=True)  17.3 us
    all_gather x1, blocking collectives, on_device(): first_rows = jnp.concatenate(lax.all_gather(first_part, 'ep'), axis=1)  17.3 us
    dot_general x5, matrix products, on_device(): jnp.dot(stream, weight, preferred_element_type=jnp.float32)  4.34 us
    all_to_all x1, waiting for transfers between devices, on_device(): lax.all_to_all(expert_out, 'ep', split_axis=1, concat_axis=0, tiled=True)  4.33 us
  transfers between devices with their start and end apart: 1, of which 1 were waited for; matrix products, arithmetic and copies ran while one was open for 1% of the time, Pallas kernels for 0%

profile of v1, /device:TPU:0, one launch (start us, length us, event | category | flops | bytes accessed | tf_op | source)
XLA Modules:
  0.0 190.4 jit_solution(5041926902427607834)
XLA Ops:
  0.6 0.0 copy-start
  0.6 0.0 copy-start.6
  0.7 0.0 copy-start.7
  0.7 1.4 convolution_dynamic-update-slice_fusion.1
  2.1 0.2 convolution_dynamic-update-slice_fusion
  2.3 1.0 convolution_dynamic-update-slice_fusion.3
  3.2 1.0 convolution_dynamic-update-slice_fusion.2
  4.2 0.8 convolution_dynamic-update-slice_fusion.4
  5.0 66.2 %all-reduce.4 = bf16[16,4640]{1,0:T(8,128)(2,1)S(1)} all-reduce(f32[16,4640]{1,0:T(8,128)S(1)} %convolution_dynamic-update-slice_fusion.4), channel_id=4, replica_groups=mesh['grp'=2,'ep'=16] {'ep'}, use_global_device_ids=true, to_apply=%region_0.0.clone | all-reduce | flops 74240 | bytes 445440
  71.2 0.0 copy-start.17
  71.3 0.6 copy-done.17
  71.9 0.6 dynamic-slice
  72.5 0.7 dynamic-slice_convert_fusion
  73.2 0.0 copy-start.8
  73.2 0.0 copy-done.9
  73.2 0.7 copy-done.8
  73.9 0.1 multiply_reduce_fusion.1
  74.0 0.0 copy-start.14
  74.1 0.0 copy-start.15
  74.1 0.1 reshape.263
  74.1 0.6 copy-done.14
  74.7 0.0 copy-done.15
  74.7 0.1 broadcast_multiply_fusion
  74.8 0.0 copy-done.1
  74.8 0.0 copy-start.16
  74.8 0.0 copy-start.11
  74.9 1.4 multiply_reduce_fusion
  76.2 0.1 reduce_sum.91
  76.3 0.1 reduce_sum.90
  76.4 0.0 copy-done.16
  76.4 0.1 mul.271
  76.5 0.1 mul.272
  76.5 0.1 mul.277
  76.6 0.1 mul.273
  76.7 0.5 broadcast.167
  77.2 0.7 fusion.56
  77.9 0.1 multiply_reduce_fusion.4
  78.1 0.1 mul.281
  78.2 17.3 %all-gather = bf16[32768]{0:T(1024)(128)(2,1)S(1)} all-gather(bf16[2048]{0:T(1024)(128)(2,1)S(1)} %multiply_convert_fusion.2), channel_id=2, replica_groups=mesh['grp'=2,'ep'=16] {'ep'}, dimensions={0}, use_global_device_ids=true | all-gather | bytes 69632 | tf_op jit(solution)/shard_map/all_gather | solution.py:119
  95.5 0.0 copy-start.3
  95.5 1.3 convolution_convert_fusion.2
  96.8 0.1 fusion.42
  96.9 0.8 dynamic_slice.12
  97.7 31.4 %all-reduce.2 = (f32[16]{0:T(128)S(1)}, f32[16]{0:T(128)S(1)}) all-reduce(f32[16]{0:T(128)S(1)} %get-tuple-element.6, f32[16]{0:T(128)S(1)} %get-tuple-element.5), channel_id=1, replica_groups=mesh['grp'=2,'ep'=16] {'ep'}, use_global_device_ids=true, to_apply=%region_7.8 | all-reduce | flops 32 | bytes 256 | tf_op jit(solution)/shard_map/psum | solution.py:126
  129.1 0.1 multiply_convert_fusion.1
  129.2 17.3 %all-gather.1 = bf16[256,128]{1,0:T(8,128)(2,1)S(1)} all-gather(bf16[16,128]{1,0:T(8,128)(2,1)S(1)} %multiply_convert_fusion.1), channel_id=3, replica_groups=mesh['grp'=2,'ep'=16] {'ep'}, dimensions={0}, use_global_device_ids=true | all-gather | bytes 69632 | tf_op jit(solution)/shard_map/all_gather | solution.py:131
  146.5 0.1 convert_reduce_fusion
  146.6 0.2 fusion.41
  146.8 0.2 dynamic-slice_reduce_fusion
  147.0 0.1 convolution_convert_fusion.1
  147.2 0.2 fusion.9
  147.4 0.0 copy-start.4
  147.4 1.3 convolution_convert_fusion
  148.8 3.6 %all-to-all-start = ((bf16[8,16,128]{2,0,1:T(8,128)(2,1)}), bf16[8,16,128]{2,0,1:T(8,128)(2,1)S(1)}, u32[]{:S(2)}, u32[]{:S(2)}) async-start(bf16[8,16,128]{2,0,1:T(8,128)(2,1)} %bitcast.15), calls=%async_computation | async-start | bytes 65536 | tf_op jit(solution)/shard_map/all_to_all | solution.py:144
  152.4 0.2 fusion.13
  152.7 1.2 fusion.5
  153.9 0.6 pad_maximum_fusion
  154.5 0.0 copy-done.12
  154.6 0.1 select_reduce_fusion
  154.7 4.3 %all-to-all-done = bf16[8,16,128]{2,0,1:T(8,128)(2,1)S(1)} async-done(((bf16[8,16,128]{2,0,1:T(8,128)(2,1)}), bf16[8,16,128]{2,0,1:T(8,128)(2,1)S(1)}, u32[]{:S(2)}, u32[]{:S(2)}) %all-to-all-start) | async-done | bytes 32800 | tf_op jit(solution)/shard_map/all_to_all | solution.py:144
  159.0 0.4 fusion.54
  159.3 29.7 %all-reduce.1 = (f32[16]{0:T(128)S(1)}, f32[16]{0:T(128)S(1)}) all-reduce(f32[16]{0:T(128)S(1)} %get-tuple-element.4, f32[16]{0:T(128)S(1)} %get-tuple-element.3), channel_id=1, replica_groups=mesh['grp'=2,'ep'=16] {'ep'}, use_global_device_ids=true, to_apply=%region_14.15 | all-reduce | flops 32 | bytes 256 | tf_op jit(solution)/shard_map/psum | solution.py:159
  189.0 0.7 copy-done.13
  189.7 0.7 multiply_convert_fusion
  (34 shorter events, 0.3 us)
Async XLA Ops:
  0.6 146.8 %copy-start = (bf16[1,256,2048]{2,1,0:T(8,128)(2,1)S(1)}, bf16[1,256,2048]{2,1,0:T(8,128)(2,1)}, u32[]{:S(2)}) copy-start(bf16[1,256,2048]{2,1,0:T(8,128)(2,1)} %param.43) | copy-start | bytes 3145732
  0.6 1.4 copy-start.6
  0.7 1.4 copy-start.7
  0.7 74.1 %copy-start.1 = (f32[1,32,64,128]{3,2,1,0:T(8,128)S(1)}, f32[1,32,64,128]{3,2,1,0:T(8,128)}, u32[]{:S(2)}) copy-start(f32[1,32,64,128]{3,2,1,0:T(8,128)} %param.26) | copy-start | bytes 3145732
  71.2 0.7 copy-start.17
  72.5 0.7 copy-start.9
  73.2 0.7 copy-start.8
  74.0 0.7 copy-start.14
  74.1 0.7 copy-start.15
  74.8 1.5 copy-start.16
  74.8 3.3 %copy-start.11 = (f32[2048]{0:T(1024)S(1)}, f32[2048]{0:T(1024)}, u32[]{:S(2)}) copy-start(f32[2048]{0:T(1024)} %param.36) | copy-start | bytes 24580
  76.2 70.9 %copy-start.2 = (bf16[1,2048,256]{2,1,0:T(8,128)(2,1)S(1)}, bf16[1,2048,256]{2,1,0:T(8,128)(2,1)}, u32[]{:S(2)}) copy-start(bf16[1,2048,256]{2,1,0:T(8,128)(2,1)} %param.41) | copy-start | bytes 3145732
  95.5 51.1 %copy-start.10 = (s32[16,4]{0,1:T(4,128)S(1)}, s32[16,4]{0,1:T(4,128)}, u32[]{:S(2)}) copy-start(s32[16,4]{0,1:T(4,128)} %param.39) | copy-start | bytes 772
  95.5 51.9 %copy-start.3 = (bf16[1,2048,256]{2,1,0:T(8,128)(2,1)S(1)}, bf16[1,2048,256]{2,1,0:T(8,128)(2,1)}, u32[]{:S(2)}) copy-start(bf16[1,2048,256]{2,1,0:T(8,128)(2,1)} %param.42) | copy-start | bytes 3145732
  147.4 5.0 %copy-start.4 = (bf16[2048,256]{1,0:T(8,128)(2,1)S(1)}, bf16[2048,256]{1,0:T(8,128)(2,1)}, u32[]{:S(2)}) copy-start(bf16[2048,256]{1,0:T(8,128)(2,1)} %param.44) | copy-start | bytes 3145732
  148.8 3.9 %copy-start.5 = (bf16[2048,256]{1,0:T(8,128)(2,1)S(1)}, bf16[2048,256]{1,0:T(8,128)(2,1)}, u32[]{:S(2)}) copy-start(bf16[2048,256]{1,0:T(8,128)(2,1)} %param.45) | copy-start | bytes 3145732
  148.8 10.2 %all-to-all-start = ((bf16[8,16,128]{2,0,1:T(8,128)(2,1)}), bf16[8,16,128]{2,0,1:T(8,128)(2,1)S(1)}, u32[]{:S(2)}, u32[]{:S(2)}) async-start(bf16[8,16,128]{2,0,1:T(8,128)(2,1)} %bitcast.15), calls=%async_computation | async-start | bytes 65536 | tf_op jit(solution)/shard_map/all_to_all | solution.py:144
  153.9 0.7 copy-start.12
  189.0 0.7 copy-start.13
